TPU v7x, 512 devices: a whole 4x4x16 slice. The times are simulated.
512 devices in a mesh: kv: 64 (over z, y), tp: 8 (over x, core).
Axes of the slice: x: 4, y: 4, z: 16, core: 2. Of those that a mesh axis runs over, the one named last changes fastest.
Arguments:
- tokens: bfloat16 [256, 4096], P(None, 'kv'), may hold values from -12 to 12
- mix_gain: float32 [4096], P('kv'), may hold values from 0.1 to 1.9
- w_query: bfloat16 [4096, 2048], P('kv', 'tp'), may hold values from -0.09375 to 0.09375
- w_key: bfloat16 [4096, 2048], P('kv', 'tp'), may hold values from -0.09375 to 0.09375
- w_value: bfloat16 [4096, 2048], P('kv', 'tp'), may hold values from -0.09375 to 0.09375
- w_gate: bfloat16 [4096, 2048], P('kv', 'tp'), may hold values from -0.09375 to 0.09375
- w_beta: bfloat16 [4096, 16], P('kv', 'tp'), may hold values from -0.09375 to 0.09375
- w_decay: bfloat16 [4096, 16], P('kv', 'tp'), may hold values from -0.09375 to 0.09375
- decay_rate: float32 [16], P('tp'), may hold values from 0.05 to 3
- head_gain: float32 [128], replicated, may hold values from 0.1 to 1.9
- state: float32 [256, 16, 128, 128], P('kv', 'tp'), may hold values from -1.2 to 1.2
- w_out: bfloat16 [2048, 4096], P('tp', 'kv'), may hold values from -0.25 to 0.25
- mlp_gain: float32 [4096], P('kv'), may hold values from 0.1 to 1.9
- w_up: bfloat16 [4096, 16384], P('kv', 'tp'), may hold values from -0.09375 to 0.09375
- w_down: bfloat16 [16384, 4096], P('tp', 'kv'), may hold values from -0.046875 to 0.046875
Outputs:
- layer_out: bfloat16 [256, 4096], P(None, 'kv')
- new_state: float32 [256, 16, 128, 128], P('kv', 'tp')
All inputs are finite; a program needn't handle non-finite values.
Results may differ from a plain program's by a relative error of at most 0.017.
Values may be sent and summed in bfloat16 or wider, within the bound.
A program may use at most 64 MiB of HBM per device.

v0:
```python
import jax
import jax.numpy as jnp
from jax import lax
from jax.sharding import Mesh
from jax.sharding import PartitionSpec as P

D = 4096
KV = ("kv_0", "kv_1")


norm_eps = 1e-06


def in_blocks(x, dim, length):
    shape = x.shape
    pieces = x.reshape(*shape[:dim], length, shape[dim] // length, *shape[dim + 1 :])
    return jnp.moveaxis(pieces, dim, 0)


def summed_on_arrival(x, axis, dim):
    length = lax.axis_size(axis)
    pieces = lax.all_to_all(in_blocks(x, dim, length), axis, 0, 0, tiled=True)
    return jnp.sum(pieces.astype(jnp.float32), axis=0)


def side_by_side(arrays, axis, dim, along):
    columns = [a.reshape(*a.shape[:along], -1) for a in arrays]
    both = jnp.concatenate(columns, axis=along)
    out, at, gathered = (summed_on_arrival(both, axis, dim), 0, [])
    for a, column in zip(arrays, columns):
        share = out[..., at : at + column.shape[along]]
        gathered.append(share.reshape(*share.shape[:along], *a.shape[along:]))
        at += column.shape[along]
    return tuple(gathered)


def laid_out(pieces, dim):
    shape = list(pieces.shape[1:])
    shape[dim] *= pieces.shape[0]
    return jnp.moveaxis(pieces, 0, dim).reshape(shape)


def copy_for_each(x, axis):
    copies = jnp.broadcast_to(x, (lax.axis_size(axis), *x.shape))
    return lax.all_to_all(copies, axis, split_axis=0, concat_axis=0, tiled=True)


def collect(x, axis, dim):
    return laid_out(copy_for_each(x, axis), dim)


def over_copies(x, axis):
    everything = copy_for_each(x, axis)
    return jnp.sum(everything.astype(jnp.float32), axis=0)


def gather_axes(x, axes, dim):
    if not axes:
        return x
    nearer = lax.all_gather(x, axes[-1], axis=dim, tiled=True)
    return gather_axes(nearer, axes[:-1], dim)


def rms_scale(values):
    return lax.rsqrt(jnp.mean(values * values, axis=-1, keepdims=True) + norm_eps)


def delta_update(
    query_pre, key_pre, value_pre, gate_pre, beta_pre, decay_pre, decay_rate, head_gain, state
):
    query = jax.nn.silu(query_pre)
    query = (
        query
        * lax.rsqrt(jnp.sum(query * query, axis=-1, keepdims=True) + norm_eps)
        * query.shape[-1] ** (-0.5)
    )
    keyed = jax.nn.silu(key_pre)
    keyed = keyed * lax.rsqrt(jnp.sum(keyed * keyed, axis=-1, keepdims=True) + norm_eps)
    valued = jax.nn.silu(value_pre)
    beta = jax.nn.sigmoid(beta_pre)
    decay = jnp.exp(-decay_rate * jax.nn.softplus(decay_pre))
    recalled = jnp.einsum("bhk,bhkv->bhv", keyed, state, precision=lax.Precision.HIGHEST)
    corrected = state - beta[:, :, None, None] * keyed[:, :, :, None] * recalled[:, :, None, :]
    new_state = (
        decay[:, :, None, None] * corrected
        + beta[:, :, None, None] * keyed[:, :, :, None] * valued[:, :, None, :]
    )
    read = jnp.einsum("bhkv,bhk->bhv", new_state, query, precision=lax.Precision.HIGHEST)
    mixed = read * rms_scale(read) * head_gain * jax.nn.silu(gate_pre)
    return (mixed, new_state)


def body(
    tokens,
    mix_gain,
    w_query,
    w_key,
    w_value,
    w_gate,
    w_beta,
    w_decay,
    decay_rate,
    head_gain,
    state,
    w_out,
    mlp_gain,
    w_up,
    w_down,
):
    f32 = jnp.float32
    bf16 = jnp.bfloat16
    local_rows = state.shape[0]
    heads_here = state.shape[1]
    head_size = state.shape[2]
    tok32 = tokens.astype(f32)
    squares = jnp.sum(tok32 * tok32, axis=1)
    gained = (tok32 * mix_gain).astype(bf16)
    joined = jnp.concatenate([w_query, w_key, w_value, w_gate], axis=1)
    rate_weights = jnp.concatenate([w_beta, w_decay], axis=1)
    main_term = jnp.dot(gained, joined, preferred_element_type=f32)
    rate_term = jnp.dot(gained, rate_weights, preferred_element_type=f32)
    main_part, rate_part, energy = side_by_side(
        (
            main_term.astype(jnp.bfloat16),
            rate_term.astype(jnp.bfloat16),
            squares.astype(jnp.bfloat16),
        ),
        KV,
        0,
        1,
    )
    scale = lax.rsqrt(energy / D + norm_eps)[:, None]
    main_part = (main_part * scale).reshape(local_rows, 4, heads_here, head_size)
    rate_part = rate_part * scale
    mixed, new_state = delta_update(
        main_part[:, 0],
        main_part[:, 1],
        main_part[:, 2],
        main_part[:, 3],
        rate_part[:, :heads_here],
        rate_part[:, heads_here:],
        decay_rate,
        head_gain,
        state,
    )
    mixed = mixed.reshape(local_rows, heads_here * head_size).astype(bf16)
    head_term = jnp.dot(collect(mixed, KV, 0), w_out, preferred_element_type=f32)
    attended = over_copies(head_term.astype(jnp.bfloat16), "tp").astype(jnp.float32)
    residual = lax.optimization_barrier((tok32 + attended).astype(bf16)).astype(f32)
    squares_mid = jnp.sum(residual * residual, axis=1)
    gained_mid = (residual * mlp_gain).astype(bf16)
    up_term = jnp.dot(gained_mid, w_up, preferred_element_type=f32)
    up_part, energy_mid = side_by_side(
        (up_term.astype(jnp.bfloat16), squares_mid.astype(jnp.bfloat16)), KV, 0, 1
    )
    scaled = up_part * lax.rsqrt(energy_mid / D + norm_eps)[:, None]
    down_term = jnp.dot(
        gather_axes(jnp.square(jax.nn.relu(scaled)).astype(bf16), KV, 0),
        w_down,
        preferred_element_type=f32,
    )
    mixer = over_copies(down_term.astype(jnp.bfloat16), "tp").astype(jnp.float32)
    layer_out = (residual + mixer).astype(bf16)
    return (layer_out, new_state)


def solution(mesh):
    finer = Mesh(mesh.devices.reshape(16, 4, mesh.shape["tp"]), ("kv_0", "kv_1", "tp"))
    return jax.shard_map(
        body,
        mesh=finer,
        in_specs=(
            P(None, KV),
            P(KV),
            P(KV, "tp"),
            P(KV, "tp"),
            P(KV, "tp"),
            P(KV, "tp"),
            P(KV, "tp"),
            P(KV, "tp"),
            P("tp"),
            P(),
            P(KV, "tp", None, None),
            P("tp", KV),
            P(KV),
            P(KV, "tp"),
            P("tp", KV),
        ),
        out_specs=(P(None, KV), P(KV, "tp", None, None)),
        check_vma=False,
    )
```

profile of v0, /device:TPU:1, one launch (start us, length us, event | category | flops | bytes accessed | tf_op | source)
XLA Modules:
  0.0 262.4 jit_solution(638212230143182629)
XLA Ops:
  7.2 0.8 fusion.8
  8.0 1.0 convolution_convert_fusion.4
  9.0 0.1 copy.64
  9.1 0.2 convert_element_type.104
  9.4 1.2 convolution_convert_fusion.1
  10.6 0.2 concatenate.21
  10.8 1.9 concatenate.24
  12.7 19.4 %all-to-all-start = ((bf16[64,4,1029]{2,1,0:T(4,128)(2,1)}), bf16[64,4,1029]{2,1,0:T(4,128)(2,1)S(1)}, u32[]{:S(2)}, u32[]{:S(2)}) async-start(bf16[64,4,1029]{2,1,0:T(4,128)(2,1)} %concatenate.24), calls=%async_computation | async-start | bytes 1179648 | tf_op jit(solution)/shard_map/all_to_all | solution.py:22
  32.2 33.1 %all-to-all-done = bf16[64,4,1029]{2,1,0:T(4,128)(2,1)S(1)} async-done(((bf16[64,4,1029]{2,1,0:T(4,128)(2,1)}), bf16[64,4,1029]{2,1,0:T(4,128)(2,1)S(1)}, u32[]{:S(2)}, u32[]{:S(2)}) %all-to-all-start) | async-done | bytes 526880 | tf_op jit(solution)/shard_map/all_to_all | solution.py:22
  65.3 0.3 convert_reduce_fusion.1
  65.6 0.2 fusion.36
  65.9 0.1 multiply_reduce_fusion
  66.2 0.1 multiply_bitcast_fusion
  66.4 0.5 fusion.26
  67.0 0.2 multiply_add_fusion
  67.2 0.6 fusion.24
  68.0 22.2 %all_to_all.25 = bf16[64,4,256]{2,1,0:T(4,128)(2,1)S(1)} all-to-all(bf16[64,4,256]{2,1,0:T(4,128)(2,1)S(1)} %broadcast_in_dim.6), channel_id=1, replica_groups=mesh['kv_0'=16,'kv_1'=4,'tp'=8] {'kv_0','kv_1'}, dimensions={0} | all-to-all | bytes 262144 | tf_op jit(solution)/shard_map/all_to_all | solution.py:45
  90.3 0.2 convolution_convert_fusion.3
  90.5 14.2 %all_to_all.26 = bf16[8,256,64]{1,2,0:T(8,128)(2,1)S(1)} all-to-all(bf16[8,256,64]{1,2,0:T(8,128)(2,1)S(1)} %broadcast_in_dim.7), channel_id=1, replica_groups=mesh['kv_0'=16,'kv_1'=4,'tp'=8] {'tp'}, dimensions={0} | all-to-all | bytes 524288 | tf_op jit(solution)/shard_map/all_to_all | solution.py:45
  104.8 0.2 convert_element_type.105
  105.0 0.5 convolution_convert_fusion
  105.6 0.4 concatenate.25
  106.0 0.6 pad_maximum_fusion
  106.6 58.3 %all_to_all.27 = bf16[64,4,2049]{2,1,0:T(4,128)(2,1)S(1)} all-to-all(bf16[64,4,2049]{2,1,0:T(4,128)(2,1)S(1)} %pad_maximum_fusion), channel_id=1, replica_groups=mesh['kv_0'=16,'kv_1'=4,'tp'=8] {'kv_0','kv_1'}, dimensions={0} | all-to-all | bytes 2098176 | tf_op jit(solution)/shard_map/all_to_all | solution.py:22
  164.9 0.5 convert_reduce_fusion
  165.4 0.1 fusion.33
  165.6 10.0 %all-gather = bf16[4,4,2048]{2,1,0:T(4,128)(2,1)S(1)} all-gather(bf16[1,4,2048]{2,1,0:T(4,128)(2,1)S(1)} %fusion.18), channel_id=1, replica_groups=mesh['kv_0'=16,'kv_1'=4,'tp'=8] {'kv_1'}, dimensions={0}, use_global_device_ids=true | all-gather | bytes 81920 | tf_op jit(solution)/shard_map/all_gather | solution.py:60
  175.6 0.6 reshape.106
  176.3 55.4 %all-gather.3.cloned.1.call-done = bf16[256,2048]{1,0:T(8,128)(2,1)} async-done(((bf16[16,2048]{1,0:T(8,128)(2,1)}), bf16[256,2048]{1,0:T(8,128)(2,1)}) %all-gather.3.cloned.1.call-update) | async-done | bytes 1048592 | tf_op jit(solution)/shard_map/all_gather | solution.py:60
  231.7 1.7 convolution_convert_fusion.2
  233.4 21.5 %all_to_all.28 = bf16[8,256,64]{1,2,0:T(8,128)(2,1)S(1)} all-to-all(bf16[8,256,64]{1,2,0:T(8,128)(2,1)S(1)} %broadcast_in_dim.8), channel_id=1, replica_groups=mesh['kv_0'=16,'kv_1'=4,'tp'=8] {'tp'}, dimensions={0} | all-to-all | bytes 524288 | tf_op jit(solution)/shard_map/all_to_all | solution.py:45
  255.0 0.6 fusion.12
  (42 shorter events, 1.1 us)
Async XLA Ops:
  7.2 97.9 %copy-start = (bf16[64,2048]{1,0:T(8,128)(2,1)S(1)}, bf16[64,2048]{1,0:T(8,128)(2,1)}, u32[]{:S(2)}) copy-start(bf16[64,2048]{1,0:T(8,128)(2,1)} %param.28) | copy-start | bytes 786436
  10.8 21.4 %copy-start.8 = (f32[2]{0:T(128)S(1)}, f32[2]{0:T(128)}, u32[]{:S(2)}) copy-start(f32[2]{0:T(128)} %param.23) | copy-start | bytes 28
  12.7 53.7 %copy-start.1 = (f32[4,2,128,128]{3,2,1,0:T(8,128)S(1)}, f32[4,2,128,128]{3,2,1,0:T(8,128)}, u32[]{:S(2)}) copy-start(f32[4,2,128,128]{3,2,1,0:T(8,128)} %param.25) | copy-start | bytes 1572868
  12.7 52.6 %all-to-all-start = ((bf16[64,4,1029]{2,1,0:T(4,128)(2,1)}), bf16[64,4,1029]{2,1,0:T(4,128)(2,1)S(1)}, u32[]{:S(2)}, u32[]{:S(2)}) async-start(bf16[64,4,1029]{2,1,0:T(4,128)(2,1)} %concatenate.24), calls=%async_computation | async-start | bytes 1179648 | tf_op jit(solution)/shard_map/all_to_all | solution.py:22
  32.1 199.6 %all-gather.3.cloned.1.call-start = ((), (), s32[]{:S(2)}) async-start(), calls=%async_computation.5 | async-start | bytes 1114112 | tf_op jit(solution)/shard_map/all_gather | solution.py:60
  66.0 1.9 copy-start.7
  67.0 23.3 %copy-start.5 = (bf16[256,64]{0,1:T(8,128)(2,1)S(1)}, bf16[256,64]{0,1:T(8,128)(2,1)}, u32[]{:S(2)}) copy-start(bf16[256,64]{0,1:T(8,128)(2,1)} %param.26) | copy-start | bytes 98308
  67.2 37.5 %copy-start.2 = (f32[4,2,128,128]{3,2,1,0:T(8,128)}, f32[4,2,128,128]{3,2,1,0:T(8,128)S(1)}, u32[]{:S(2)}) copy-start(f32[4,2,128,128]{3,2,1,0:T(8,128)S(1)} %multiply_add_fusion) | copy-start | bytes 1572868
  67.8 36.9 %copy-start.3 = (bf16[256,64]{0,1:T(8,128)(2,1)S(1)}, bf16[256,64]{0,1:T(8,128)(2,1)}, u32[]{:S(2)}) copy-start(bf16[256,64]{0,1:T(8,128)(2,1)} %param.15) | copy-start | bytes 98308
  68.0 37.1 %copy-start.6 = (f32[64]{0:T(128)S(1)}, f32[64]{0:T(128)}, u32[]{:S(2)}) copy-start(f32[64]{0:T(128)} %param.27) | copy-start | bytes 772
  164.9 66.8 %copy-start.4 = (bf16[2048,64]{0,1:T(8,128)(2,1)S(1)}, bf16[2048,64]{0,1:T(8,128)(2,1)}, u32[]{:S(2)}) copy-start(bf16[2048,64]{0,1:T(8,128)(2,1)} %param.29) | copy-start | bytes 786436
Sparse Core Ops, SparseCore 0:
  176.4 55.2 all-gather.2
where the time goes:
time: 263 us; the launch traced here: 262 us
  blocking collectives  126 us (48%)
  waiting for transfers between devices  88.6 us (34%)
  starting transfers between devices  19.4 us (7%)
  between operations  14.3 us (5%)
  matrix products  5.61 us (2%)
  other arithmetic  4.18 us (2%)
  local copies, waits for them, and re-layouts  4.08 us (2%)
    all_to_all x1, blocking collectives, summed_on_arrival(): pieces = lax.all_to_all(in_blocks(x, dim, length), axis, 0, 0, tiled=True)  58.3 us
    all_to_all x3, blocking collectives, copy_for_each(): return lax.all_to_all(copies, axis, split_axis=0, concat_axis=0, tiled=True)  57.9 us
    all_gather x1, waiting for transfers between devices, gather_axes(): nearer = lax.all_gather(x, axes[-1], axis=dim, tiled=True)  55.4 us
    all_to_all x1, waiting for transfers between devices, summed_on_arrival(): pieces = lax.all_to_all(in_blocks(x, dim, length), axis, 0, 0, tiled=True)  33.1 us
    all_to_all x1, starting transfers between devices, summed_on_arrival(): pieces = lax.all_to_all(in_blocks(x, dim, length), axis, 0, 0, tiled=True)  19.4 us
    all_gather x1, blocking collectives, gather_axes(): nearer = lax.all_gather(x, axes[-1], axis=dim, tiled=True)  10 us
  transfers between devices with their start and end apart: 2, of which 2 were waited for; matrix products, arithmetic and copies ran while one was open for 0% of the time, Pallas kernels for 0%

commit v1 on v0

v1 whole, which is shorter than its diff:
```python
import functools

import jax
import jax.numpy as jnp
from jax import lax
from jax.experimental import pallas as pl
from jax.experimental.pallas import tpu as pltpu
from jax.sharding import PartitionSpec as P

D = 4096
EPS = 1e-06
MESH = pl.DeviceIdType.MESH
F32 = jnp.float32
BF16 = jnp.bfloat16
NZ, NY, NT = 16, 4, 8
FAR_FIRST = (8, 7, 9, 6, 10, 5, 11, 4, 12, 3, 13, 2, 14, 1, 15)

NN = (((1,), (0,)), ((), ()))
NT_DIMS = (((1,), (1,)), ((), ()))


def mm(a, b, dims=NN):
    return lax.dot_general(a, b, dims, preferred_element_type=F32)


def iota(shape, dim):
    return lax.broadcasted_iota(jnp.int32, shape, dim)


def one_hot(cond):
    return jnp.where(cond, 1.0, 0.0).astype(BF16)


class Wire:
    def __init__(self, send_sem, recv_sem):
        self.send_sem, self.recv_sem = send_sem, recv_sem
        self.count, self.sent = 0, []

    def send(self, src, dst, landed, kv, tp):
        k = self.count
        self.count += 1
        copy = pltpu.make_async_remote_copy(
            src, dst, self.send_sem.at[k], self.recv_sem.at[k],
            device_id={"kv": kv, "tp": tp}, device_id_type=MESH,
        )
        copy.start()
        self.sent.append(copy)
        return pltpu.make_async_remote_copy(
            src, landed, self.send_sem.at[k], self.recv_sem.at[k],
            device_id={"kv": kv, "tp": tp}, device_id_type=MESH,
        )

    def finish(self):
        for copy in self.sent:
            copy.wait_send()


def kernel(
    tok_ref, mixg_ref, wq_ref, wk_ref, wv_ref, wg_ref, small_ref, rate_ref, hgain_ref,
    state_ref, wo_ref, mlpg_ref, wu_ref, wd_ref,
    out_ref, new_ref,
    wqf, wkf, wvf, wgf, wof, wuf, wdf, st, stn,
    tg_s, tg, sm, mg, sa, sb, ra, rb, mx, at, ru_s, ru, hid, res_s, res, fin_s, fin, rd,
    onehots, send_sem, recv_sem, local_sem,
):
    kv, tp = lax.axis_index("kv"), lax.axis_index("tp")
    z, y = kv // NY, kv % NY

    def kv_of(zz, yy):
        return zz * NY + yy

    def zp(d):
        return (z + d) % NZ

    def yp(d):
        return (y + d) % NY

    def tq(d):
        return (tp + d) % NT

    barrier = pltpu.get_barrier_semaphore()
    for d in range(1, NZ):
        pl.semaphore_signal(barrier, 1, device_id={"kv": kv_of(zp(d), y), "tp": tp}, device_id_type=MESH)
    for d in range(1, NY):
        pl.semaphore_signal(barrier, 1, device_id={"kv": kv_of(z, yp(d)), "tp": tp}, device_id_type=MESH)
    for e in range(NY):
        for d in range(1, NT):
            pl.semaphore_signal(barrier, 1, device_id={"kv": kv_of(z, yp(e)), "tp": tq(d)}, device_id_type=MESH)

    loads = []
    for i, (src, dst) in enumerate((
        (wq_ref, wqf.at[y]), (wk_ref, wkf.at[y]), (wv_ref, wvf.at[y]), (wg_ref, wgf.at[y]),
        (wo_ref, wof.at[y]), (wu_ref, wuf.at[y]), (wd_ref, wdf.at[y]), (state_ref, st),
    )):
        load = pltpu.make_async_copy(src, dst, local_sem.at[i])
        load.start()
        loads.append(load)

    r64, c64 = iota((64, 64), 0), iota((64, 64), 1)
    eye64 = one_hot(r64 == c64)
    gain_col = jnp.sum(jnp.where(r64 == c64, jnp.broadcast_to(mixg_ref[...], (64, 64)), 0.0), axis=1, keepdims=True)
    tokt = tok_ref[...]
    gnt = (tokt.astype(F32) * gain_col).astype(BF16)
    rr, cc = iota((256, 128), 0), iota((256, 128), 1)
    cl = cc % 64
    for yy in range(NY):
        row_of = 16 * (cl // 4) + 4 * yy + cl % 4
        hit = rr == row_of
        pick_t = one_hot(hit & (cc < 64))
        pick_g = one_hot(hit & (cc >= 64))
        tg_s[yy] = (mm(tokt, pick_t) + mm(gnt, pick_g)).astype(BF16)
    lane = iota((8, 256), 1)
    mg[pl.ds(y, 1)] = jnp.where(lane // 64 == y, jnp.broadcast_to(mlpg_ref[...], (8, 256)), 0.0)[None]
    sm[pl.ds(y, 1)] = small_ref[...][None]
    tg[pl.ds(y, 1)] = tg_s[pl.ds(y, 1)]

    rr, cc = iota((128, 128), 0), iota((128, 128), 1)
    src_row = 4 * (rr // 8) + rr % 4
    half = (rr % 8) // 4
    q_g = [one_hot((cc == 64 + src_row) & (half == h)) for h in range(2)]
    q_t = one_hot(cc == src_row)
    rr2, cc2 = iota((64, 128), 0), iota((64, 128), 1)
    pick_tok = one_hot(cc2 == rr2)
    for h in range(2):
        onehots[h] = one_hot(cc2 == 8 * (rr2 // 4) + 4 * h + rr2 % 4)

    wire = Wire(send_sem, recv_sem)
    pl.semaphore_wait(barrier, (NZ - 1) + (NY - 1) + NY * (NT - 1))

    def y_send(buf, d):
        return wire.send(buf.at[y], buf.at[y], buf.at[yp(-d)], kv_of(z, yp(d)), tp)

    got = []
    for d in (1, 3, 2):
        got.append(wire.send(tg_s.at[yp(d)], tg.at[y], tg.at[yp(-d)], kv_of(z, yp(d)), tp))
        got.append(y_send(sm, d))
        got.append(y_send(mg, d))
    for i in range(4):
        loads[i].wait()
    full = (wqf, wkf, wvf, wgf)
    right, left = [None] * 4, [None] * 4
    relay = [None] * 4
    for pair in ((0, 1), (2, 3)):
        for i in pair:
            right[i] = y_send(full[i], 1)
            left[i] = y_send(full[i], 3)
        a, b = pair
        right[a].wait_recv()
        relay[a] = wire.send(full[a].at[yp(-1)], full[a].at[yp(-1)], full[a].at[yp(-2)], kv_of(z, yp(1)), tp)
        left[b].wait_recv()
        relay[b] = wire.send(full[b].at[yp(1)], full[b].at[yp(1)], full[b].at[yp(2)], kv_of(z, yp(-1)), tp)
    loads[4].wait()
    loads[5].wait()
    loads[6].wait()
    wo_got = [y_send(wof, d) for d in (1, 3, 2)]
    wu_got = [y_send(wuf, d) for d in (1, 3)]

    for g in got:
        g.wait_recv()
    tgv = tg[...].reshape(256, 128)
    lq = [mm(q_g[h], tgv, NT_DIMS).astype(BF16) for h in range(2)]
    tok_rows = mm(pick_tok, tgv, NT_DIMS)

    t32 = tgv.astype(F32)
    energy = jnp.sum(t32 * t32, axis=0, keepdims=True)
    e_hi = energy.astype(BF16)
    e_lo = (energy - e_hi.astype(F32)).astype(BF16)
    e_rows = jnp.where(rr == 2, jnp.broadcast_to(e_hi.astype(F32), (128, 128)),
                       jnp.where(rr == 3, jnp.broadcast_to(e_lo.astype(F32), (128, 128)), 0.0)).astype(BF16)
    small_out = mm(q_t, e_rows, NT_DIMS)
    for h in range(2):
        sel = one_hot(((iota((128, 8), 0) == 0) & (iota((128, 8), 1) == h))
                      | ((iota((128, 8), 0) == 1) & (iota((128, 8), 1) == 2 + h)))
        parts = [mm(eye64, mm(sel, sm[yy][:, :64]).astype(BF16), NT_DIMS) for yy in range(NY)]
        w_small = jnp.concatenate(parts, axis=0).astype(BF16)
        small_out += mm(lq[h], w_small)

    def project(buf):
        w = buf[...].reshape(256, 256)
        return mm(lq[0], w[:, :128]) + mm(lq[1], w[:, 128:])

    def stage(blocks):
        return jnp.concatenate([b.reshape(NZ, 8, 128) for b in blocks], axis=1).astype(BF16)

    def z_scatter(src, dst):
        return [wire.send(src.at[zp(d)], dst.at[z], dst.at[zp(-d)], kv_of(zp(d), y), tp) for d in FAR_FIRST]

    for i, which in ((0, relay), (1, relay)):
        which[i].wait_recv()
    left[0].wait_recv()
    right[1].wait_recv()
    staged = stage([project(wqf), project(wkf), small_out])
    sa[...] = staged
    got_a = z_scatter(sa, ra)
    relay[2].wait_recv()
    relay[3].wait_recv()
    left[2].wait_recv()
    right[3].wait_recv()
    sb[...] = stage([project(wvf), project(wgf)])
    got_b = z_scatter(sb, rb)
    ra[pl.ds(z, 1)] = sa[pl.ds(z, 1)]
    rb[pl.ds(z, 1)] = sb[pl.ds(z, 1)]
    loads[7].wait()
    for g in got_a:
        g.wait_recv()
    sum_a = jnp.sum(ra[...].astype(F32), axis=0)
    extra = sum_a[16:24]
    scale = lax.rsqrt((extra[:, 2:3] + extra[:, 3:4]) * (1.0 / D) + EPS)
    query = jax.nn.silu(sum_a[0:8] * scale)
    query = query * lax.rsqrt(jnp.sum(query * query, axis=1, keepdims=True) + EPS) * (128 ** -0.5)
    keyed = jax.nn.silu(sum_a[8:16] * scale)
    keyed = keyed * lax.rsqrt(jnp.sum(keyed * keyed, axis=1, keepdims=True) + EPS)
    beta = jax.nn.sigmoid(extra[:, 0:1] * scale)
    decay = jnp.exp(-rate_ref[:, 0:1] * jax.nn.softplus(extra[:, 1:2] * scale))
    key_t = jnp.transpose(keyed)
    query_t = jnp.transpose(query)
    recs = []
    for b in range(8):
        h, i = b // 4, b % 4
        recs.append(jnp.sum(st[i, h] * key_t[:, b:b + 1], axis=0, keepdims=True))
    recalled = jnp.concatenate(recs, axis=0)
    for g in got_b:
        g.wait_recv()
    sum_b = jnp.sum(rb[...].astype(F32), axis=0)
    valued = jax.nn.silu(sum_b[0:8] * scale)
    gate = jax.nn.silu(sum_b[8:16] * scale)
    write = beta * (valued - decay * recalled)
    reads = []
    for b in range(8):
        h, i = b // 4, b % 4
        fresh = decay[b:b + 1, :] * st[i, h] + key_t[:, b:b + 1] * write[b:b + 1, :]
        stn[i, h] = fresh
        reads.append(jnp.sum(fresh * query_t[:, b:b + 1], axis=0, keepdims=True))
    read = jnp.concatenate(reads, axis=0)
    mixed = read * lax.rsqrt(jnp.mean(read * read, axis=1, keepdims=True) + EPS) * hgain_ref[...] * gate
    mx[pl.ds(z, 1)] = mixed.astype(BF16)[None]

    def z_gather(buf):
        return [wire.send(buf.at[z], buf.at[z], buf.at[zp(-d)], kv_of(zp(d), y), tp) for d in FAR_FIRST]

    got_m = z_gather(mx)
    store = pltpu.make_async_copy(stn, new_ref, local_sem.at[8])
    store.start()
    wu_got[0].wait_recv()
    wu_got[1].wait_recv()
    wu_far = [
        wire.send(wuf.at[yp(-1), pl.ds(0, 32)], wuf.at[yp(-1), pl.ds(0, 32)], wuf.at[yp(-2), pl.ds(0, 32)], kv_of(z, yp(1)), tp),
        wire.send(wuf.at[yp(1), pl.ds(32, 32)], wuf.at[yp(1), pl.ds(32, 32)], wuf.at[yp(2), pl.ds(32, 32)], kv_of(z, yp(-1)), tp),
    ]
    wd_got = [y_send(wdf, d) for d in (1, 3)]
    for g in wo_got:
        g.wait_recv()
    for g in got_m:
        g.wait_recv()
    m = mx[...].astype(F32).reshape(128, 128).astype(BF16)
    mixed2 = jnp.concatenate([mm(onehots[h], m) for h in range(2)], axis=1).astype(BF16)
    at[pl.ds(tp, 1)] = mm(mixed2, wof[...].reshape(256, 256), NT_DIMS).astype(BF16)[None]
    got_t = [wire.send(at.at[tp], at.at[tp], at.at[tq(-d)], kv, tq(d)) for d in (4, 5, 2, 3, 6, 7, 1)]
    gain_mid = jnp.sum(mg[...], axis=0)[0:1]
    for g in got_t:
        g.wait_recv()
    attended = jnp.sum(at[...].astype(F32), axis=0)
    residual = (tok_rows + attended).astype(BF16)
    r32 = residual.astype(F32)
    gained_mid = (r32 * gain_mid).astype(BF16)
    rr3, cc3 = iota((128, 64), 0), iota((128, 64), 1)
    row3 = 4 * (rr3 // 8) + rr3 % 4
    half3 = (rr3 % 8) // 4
    em = jnp.sum(r32 * r32, axis=1, keepdims=True)
    em_hi = em.astype(BF16).astype(F32)
    em_lo = em - em_hi
    lane3 = iota((64, 128), 1)
    em_mat = jnp.where(lane3 == 0, em_hi, jnp.where(lane3 == 1, em_lo, 0.0)).astype(BF16)
    ru_s[:, :, 1024:] = mm(one_hot(cc3 == row3), em_mat).reshape(NZ, 8, 128).astype(BF16)
    lg = [mm(one_hot((cc3 == row3) & (half3 == c)), gained_mid).astype(BF16) for c in range(2)]
    for g in wu_far:
        g.wait_recv()
    wu = wuf[...].reshape(256, 2048)
    up = mm(lg[0], wu[:, :1024]) + mm(lg[1], wu[:, 1024:])
    ru_s[:, :, :1024] = up.reshape(NZ, 8, 1024).astype(BF16)
    got_u = z_scatter(ru_s, ru)
    ru[pl.ds(z, 1)] = ru_s[pl.ds(z, 1)]

    eye256 = one_hot(iota((256, 256), 0) == iota((256, 256), 1))

    def by_y(x):
        x = x.reshape(NY, 2, 32, 64)
        return jnp.concatenate([x[:, 0], x[:, 1]], axis=-1).astype(BF16)

    res_s[...] = by_y(mm(eye256, residual, NT_DIMS))
    res[pl.ds(y, 1)] = res_s[pl.ds(y, 1)]
    got_r = [wire.send(res_s.at[yp(d)], res.at[y], res.at[yp(-d)], kv_of(z, yp(d)), tp) for d in (1, 3, 2)]
    wd_got[0].wait_recv()
    wd_got[1].wait_recv()
    wd_far = [
        wire.send(wdf.at[yp(-1), pl.ds(0, 32)], wdf.at[yp(-1), pl.ds(0, 32)], wdf.at[yp(-2), pl.ds(0, 32)], kv_of(z, yp(1)), tp),
        wire.send(wdf.at[yp(1), pl.ds(32, 32)], wdf.at[yp(1), pl.ds(32, 32)], wdf.at[yp(2), pl.ds(32, 32)], kv_of(z, yp(-1)), tp),
    ]
    for g in got_u:
        g.wait_recv()
    total = jnp.sum(ru[...].astype(F32), axis=0)
    scale_mid = lax.rsqrt((total[:, 1024:1025] + total[:, 1025:1026]) * (1.0 / D) + EPS)
    hidden = jnp.square(jnp.maximum(total[:, :1024] * scale_mid, 0.0))
    hid[pl.ds(z, 1)] = hidden.astype(BF16)[None]
    got_h = z_gather(hid)
    for g in wd_far:
        g.wait_recv()
    for g in got_r:
        g.wait_recv()
    for g in got_h:
        g.wait_recv()
    hv = hid[...].astype(F32).reshape(128, 1024).astype(BF16)
    wd = wdf[...].reshape(256, 2048)
    down = None
    for c in range(2):
        rows = mm(onehots[c], hv).astype(BF16)
        term = mm(wd[:, 1024 * c:1024 * (c + 1)], rows, NT_DIMS)
        down = term if down is None else down + term
    fin_s[...] = by_y(down)
    got_f = []
    for e in (2, 1, 3, 0):
        for d in (4, 5, 2, 3, 6, 7, 1, 0):
            if e == 0 and d == 0:
                continue
            got_f.append(wire.send(
                fin_s.at[yp(e)], fin.at[tp, y], fin.at[tq(-d), yp(-e)], kv_of(z, yp(e)), tq(d)))
    fin[pl.ds(tp, 1), pl.ds(y, 1)] = fin_s[pl.ds(y, 1)][None]
    for g in got_f:
        g.wait_recv()
    mixer = jnp.sum(fin[...].astype(F32), axis=0)
    last = (res[...].astype(F32) + mixer).astype(BF16)
    flat = jnp.concatenate([last[yy] for yy in range(NY)], axis=1)
    rr4, cc4 = iota((512, 256), 0), iota((512, 256), 1)
    row4 = 16 * ((rr4 % 64) // 4) + 4 * (rr4 // 128) + rr4 % 4
    for e in range(2):
        place = one_hot((cc4 == row4) & ((rr4 % 128) // 64 == e))
        out_ref[pl.ds(32 * e, 32), :] = mm(flat, place).astype(BF16)
    store.wait()
    wire.finish()


def body(
    tokens, mix_gain, w_query, w_key, w_value, w_gate, w_beta, w_decay, decay_rate, head_gain,
    state, w_out, mlp_gain, w_up, w_down,
):
    small = jnp.concatenate([w_beta.T, w_decay.T, jnp.zeros((4, 64), BF16)], axis=0)
    small = jnp.pad(small, ((0, 0), (0, 64)))
    rate = jnp.broadcast_to(jnp.repeat(decay_rate, 4)[:, None], (8, 128))
    gain4 = jnp.concatenate([mlp_gain] * 4).reshape(1, 256)
    vmem = pl.BlockSpec(memory_space=pltpu.VMEM)
    hbm = pl.BlockSpec(memory_space=pltpu.HBM)
    v = pltpu.VMEM
    n_sem = 160
    out, new = pl.pallas_call(
        kernel,
        name="layer",
        out_shape=(
            jax.ShapeDtypeStruct((64, 256), BF16),
            jax.ShapeDtypeStruct((4, 2, 128, 128), F32),
        ),
        in_specs=[vmem, vmem, hbm, hbm, hbm, hbm, vmem, vmem, vmem, hbm, hbm, vmem, hbm, hbm],
        out_specs=(vmem, hbm),
        scratch_shapes=[
            v((4, 64, 256), BF16), v((4, 64, 256), BF16), v((4, 64, 256), BF16), v((4, 64, 256), BF16),
            v((4, 64, 256), BF16), v((4, 64, 2048), BF16), v((4, 64, 2048), BF16),
            v((4, 2, 128, 128), F32), v((4, 2, 128, 128), F32),
            v((4, 64, 128), BF16), v((4, 64, 128), BF16), v((4, 8, 128), BF16), v((4, 8, 256), F32),
            v((16, 24, 128), BF16), v((16, 16, 128), BF16), v((16, 24, 128), BF16), v((16, 16, 128), BF16),
            v((16, 8, 128), BF16), v((8, 64, 256), BF16),
            v((16, 8, 1152), BF16), v((16, 8, 1152), BF16), v((16, 8, 1024), BF16),
            v((4, 32, 128), BF16), v((4, 32, 128), BF16),
            v((4, 32, 128), BF16), v((8, 4, 32, 128), BF16), v((8, 128), F32),
            v((2, 64, 128), BF16),
            pltpu.SemaphoreType.DMA((n_sem,)), pltpu.SemaphoreType.DMA((n_sem,)),
            pltpu.SemaphoreType.DMA((9,)),
        ],
        compiler_params=pltpu.CompilerParams(
            collective_id=0, has_side_effects=True, vmem_limit_bytes=48 * 1024 * 1024,
        ),
    )(
        tokens.T, mix_gain.reshape(1, 64), w_query, w_key, w_value, w_gate, small, rate,
        head_gain.reshape(1, 128), state, w_out.T, gain4, w_up, w_down.T,
    )
    return out.T, new


def solution(mesh):
    return jax.shard_map(
        body,
        mesh=mesh,
        in_specs=(
            P(None, "kv"), P("kv"), P("kv", "tp"), P("kv", "tp"), P("kv", "tp"), P("kv", "tp"),
            P("kv", "tp"), P("kv", "tp"), P("tp"), P(), P("kv", "tp", None, None),
            P("tp", "kv"), P("kv"), P("kv", "tp"), P("tp", "kv"),
        ),
        out_specs=(P(None, "kv"), P("kv", "tp", None, None)),
        check_vma=False,
    )
```

time: 263 us -> 101 us (0.38)
  blocking collectives: 126 us -> 0 us
  waiting for transfers between devices: 88.6 us -> 0 us
  Pallas kernels: 0 us -> 88.4 us
  starting transfers between devices: 19.4 us -> 0 us
  between operations: 14.3 us -> 0.67 us
  matrix products: 5.61 us -> 0 us
  local copies, waits for them, and re-layouts: 4.08 us -> 9.69 us
    all_to_all x4 -> x0, blocking collectives: 116 us -> none  [the longest x1 58.3 us: summed_on_arrival(): pieces = lax.all_to_all(in_blocks(x, dim, length), axis, 0, 0, tiled=True)]
    pallas_call x0 -> x1, Pallas kernels: none -> 88.4 us  [body(): pl.pallas_call(kernel, name='layer', out_shape=(jax.ShapeDtypeStruct((64,...]
    all_gather x1 -> x0, waiting for transfers between devices: 55.4 us -> none  [gather_axes(): nearer = lax.all_gather(x, axes[-1], axis=dim, tiled=True)]
    all_to_all x1 -> x0, waiting for transfers between devices: 33.1 us -> none  [summed_on_arrival(): pieces = lax.all_to_all(in_blocks(x, dim, length), axis, 0, 0, tiled=True)]
    all_to_all x1 -> x0, starting transfers between devices: 19.4 us -> none  [summed_on_arrival(): pieces = lax.all_to_all(in_blocks(x, dim, length), axis, 0, 0, tiled=True)]
    all_gather x1 -> x0, blocking collectives: 10 us -> none  [gather_axes(): nearer = lax.all_gather(x, axes[-1], axis=dim, tiled=True)]
    unnamed x19 -> x24, local copies, waits for them, and re-layouts: 0.68 us -> 8.73 us
    dot_general x7 -> x0, matrix products: 5.61 us -> none  [the longest x1 1.66 us: body(): jnp.dot(gather_axes(jnp.square(jax.nn.relu(scaled)).astype(bf16), KV, 0),...]
  transfers between devices with their start and end apart: 2 -> 0, of which waited for: 2 -> 0; matrix products, arithmetic and copies ran while one was open for 0% -> 0% of each run, Pallas kernels for 0% -> 0%
where the time goes in v1:
time: 101 us; the launch traced here: 100 us
  Pallas kernels  88.4 us (88%)
  local copies, waits for them, and re-layouts  9.69 us (10%)
  other arithmetic  1.62 us (2%)
    pallas_call x1, Pallas kernels, body(): pl.pallas_call(kernel, name='layer', out_shape=(jax.ShapeDtypeStruct((64,...  88.4 us
    unnamed x24, local copies, waits for them, and re-layouts  8.73 us

profile of v1, /device:TPU:1, one launch (start us, length us, event | category | flops | bytes accessed | tf_op | source)
XLA Modules:
  0.0 100.4 jit_solution(17314330254528676090)
XLA Ops:
  0.6 0.0 copy-start.3
  0.6 0.1 pad.11.clone
  0.7 0.7 broadcast_in_dim.14
  1.4 0.1 broadcast_in_dim.15
  1.5 0.9 pad_maximum_fusion
  2.4 0.7 maximum_maximum_fusion
  3.2 0.0 copy-start.9
  3.2 0.0 copy-start.10
  3.2 0.1 broadcast_in_dim.16.rate_ref
  3.2 0.0 copy-done.3
  3.3 0.6 copy-done.9
  3.8 0.0 copy-done.10
  3.8 0.0 copy-start
  3.8 1.0 %copy-done = f32[4,2,128,128]{3,2,1,0:T(8,128)S(1)} copy-done((f32[4,2,128,128]{3,2,1,0:T(8,128)S(1)}, f32[4,2,128,128]{3,2,1,0:T(8,128)}, u32[]{:S(2)}) %copy-start) | copy-done | bytes 524312
  4.9 0.0 copy-start.1
  4.9 0.9 copy-done.1
  5.8 0.0 copy-start.2
  5.8 0.9 copy-done.2
  6.8 0.0 copy-start.4
  6.8 0.8 copy-done.4
  7.5 0.0 copy-start.5
  7.5 0.8 copy-done.5
  8.3 0.0 copy-start.6
  8.3 0.8 copy-done.6
  9.1 0.0 copy-start.7
  9.1 0.8 copy-done.7
  9.8 0.0 copy-start.8
  9.8 0.8 copy-done.8
  10.6 88.4 %layer.1 = (bf16[64,256]{1,0:T(8,128)(2,1)S(1)}, f32[4,2,128,128]{3,2,1,0:T(8,128)S(1)}) custom-call(bf16[64,256]{1,0:T(8,128)(2,1)S(1)} %bitcast.10, f32[1,64]{1,0:T(1,128)S(1)} %bitcast.14, bf16[64,256]{1,0:T(8,128)(2,1)S(1)} %copy-done.4, bf16[64,256]{1,0:T(8,128)(2,1)S(1)} %copy-done.5, bf16[64,256]{1,0:T(8,128)(2,1)S(1)} %copy-done.6, ...), custom_call_target="tpu_custom_call" | custom-call | tf_op jit(solution)/shard_map/layer/pallas_call | solution.py:354
  99.0 0.6 copy.19
  99.6 0.8 copy.20
  (2 shorter events, 0.0 us)
Async XLA Ops:
  0.6 2.6 %copy-start.3 = (bf16[256,64]{0,1:T(8,128)(2,1)S(1)}, bf16[256,64]{0,1:T(8,128)(2,1)}, u32[]{:S(2)}) copy-start(bf16[256,64]{0,1:T(8,128)(2,1)} %param.15) | copy-start | bytes 98308
  3.2 0.7 copy-start.9
  3.2 0.7 copy-start.10
  3.8 1.0 %copy-start = (f32[4,2,128,128]{3,2,1,0:T(8,128)S(1)}, f32[4,2,128,128]{3,2,1,0:T(8,128)}, u32[]{:S(2)}) copy-start(f32[4,2,128,128]{3,2,1,0:T(8,128)} %state_ref.1) | copy-start | bytes 1572868
  4.9 0.9 copy-start.1
  5.8 0.9 copy-start.2
  6.8 0.8 copy-start.4
  7.5 0.8 copy-start.5
  8.3 0.8 copy-start.6
  9.1 0.8 copy-start.7
  9.8 0.8 copy-start.8

commit v2 on v1

v2 whole, which is shorter than its diff:
```python
import functools

import jax
import jax.numpy as jnp
from jax import lax
from jax.experimental import pallas as pl
from jax.experimental.pallas import tpu as pltpu
from jax.sharding import PartitionSpec as P

D = 4096
EPS = 1e-06
MESH = pl.DeviceIdType.MESH
F32 = jnp.float32
BF16 = jnp.bfloat16
NZ, NY, NT = 16, 4, 8
FAR_FIRST = (8, 7, 9, 6, 10, 5, 11, 4, 12, 3, 13, 2, 14, 1, 15)

NN = (((1,), (0,)), ((), ()))
NT_DIMS = (((1,), (1,)), ((), ()))


def mm(a, b, dims=NN):
    return lax.dot_general(a, b, dims, preferred_element_type=F32)


def iota(shape, dim):
    return lax.broadcasted_iota(jnp.int32, shape, dim)


def one_hot(cond):
    return jnp.where(cond, 1.0, 0.0).astype(BF16)


class Group:
    def __init__(self, wire, index, name):
        self.wire, self.index, self.name, self.total = wire, index, name, None

    def copy(self, src, dst, kv, tp):
        return pltpu.make_async_remote_copy(
            src, dst, self.wire.send_sem.at[self.index], self.wire.recv_sem.at[self.index],
            device_id={"kv": kv, "tp": tp}, device_id_type=MESH,
        )

    def send(self, src, dst, kv, tp):
        self.copy(src, dst, kv, tp).start()

    def take(self, total):
        self.total = total
        with jax.named_scope(self.name):
            self.copy(total, total, self.wire.kv, self.wire.tp).wait_recv()

    def finish(self):
        self.copy(self.total, self.total, self.wire.kv, self.wire.tp).wait_send()


class Wire:
    def __init__(self, send_sem, recv_sem, kv, tp):
        self.send_sem, self.recv_sem, self.kv, self.tp = send_sem, recv_sem, kv, tp
        self.groups = []

    def group(self, name):
        self.groups.append(Group(self, len(self.groups), name))
        return self.groups[-1]

    def finish(self):
        for group in self.groups:
            group.finish()


def kernel(
    tok_ref, mixg_ref, wq_ref, wk_ref, wv_ref, wg_ref, wb_ref, wdec_ref, rate_ref, hgain_ref,
    state_ref, wo_ref, mlpg_ref, wu_ref, wd_ref,
    out_ref, new_ref,
    tokv, mixv, wbv, wdecv, ratev, hgainv, mlpv,
    wqf, wkf, wvf, wgf, wof, wuf, wdf, st,
    tg_s, tg, sm, mg, sa, sb, ra, rb, mx, at, us, near, fs, ru, hid, em, res_s, res, fin_s, fin,
    heads_in, hid_in, place, send_sem, recv_sem, local_sem,
):
    kv, tp = lax.axis_index("kv"), lax.axis_index("tp")
    z, y = kv // NY, kv % NY

    def kv_of(zz, yy):
        return zz * NY + yy

    def zp(d):
        return (z + d) % NZ

    def yp(d):
        return (y + d) % NY

    def tq(d):
        return (tp + d) % NT

    barrier = pltpu.get_barrier_semaphore()
    for d in range(1, NZ):
        pl.semaphore_signal(barrier, 1, device_id={"kv": kv_of(zp(d), y), "tp": tp}, device_id_type=MESH)
    for d in range(1, NY):
        pl.semaphore_signal(barrier, 1, device_id={"kv": kv_of(z, yp(d)), "tp": tp}, device_id_type=MESH)
    for e in range(NY):
        for d in range(1, NT):
            pl.semaphore_signal(barrier, 1, device_id={"kv": kv_of(z, yp(e)), "tp": tq(d)}, device_id_type=MESH)

    loads = []
    for i, (src, dst) in enumerate((
        (tok_ref, tokv), (mixg_ref, mixv), (wb_ref, wbv), (wdec_ref, wdecv), (mlpg_ref, mlpv),
        (rate_ref, ratev), (hgain_ref, hgainv),
        (wq_ref, wqf.at[y]), (wk_ref, wkf.at[y]), (wv_ref, wvf.at[y]), (wg_ref, wgf.at[y]),
        (wo_ref, wof.at[y]), (wu_ref, wuf.at[y]), (wd_ref, wdf.at[y]), (state_ref, st),
    )):
        load = pltpu.make_async_copy(src, dst, local_sem.at[i])
        load.start()
        loads.append(load)

    with jax.named_scope("small_loads"):
        for i in range(7):
            loads[i].wait()

    r64, c64 = iota((64, 64), 0), iota((64, 64), 1)
    eye64 = one_hot(r64 == c64)
    gain_col = jnp.sum(jnp.where(r64 == c64, jnp.broadcast_to(mixv[...], (64, 64)), 0.0), axis=1, keepdims=True)
    tokt = tokv[...]
    gnt = (tokt.astype(F32) * gain_col).astype(BF16)
    rr, cc = iota((256, 128), 0), iota((256, 128), 1)
    cl = cc % 64
    for yy in range(NY):
        row_of = 16 * (cl // 4) + 4 * yy + cl % 4
        hit = rr == row_of
        pick_t = one_hot(hit & (cc < 64))
        pick_g = one_hot(hit & (cc >= 64))
        tg_s[yy] = (mm(tokt, pick_t) + mm(gnt, pick_g)).astype(BF16)
    mg[pl.ds(y, 1)] = jnp.broadcast_to(mlpv[...], (8, 64))[None]
    wb32, wdec32 = wbv[...].astype(F32), wdecv[...].astype(F32)
    r8 = iota((8, 64), 0)
    sm_rows = jnp.zeros((8, 64), F32)
    for k, row in enumerate((wb32[0:1], wb32[1:2], wdec32[0:1], wdec32[1:2])):
        sm_rows = jnp.where(r8 == k, jnp.broadcast_to(row, (8, 64)), sm_rows)
    sm[pl.ds(y, 1)] = sm_rows.astype(BF16)[None]
    tg[pl.ds(y, 1)] = tg_s[pl.ds(y, 1)]

    rr, cc = iota((128, 128), 0), iota((128, 128), 1)
    src_row = 4 * (rr // 8) + rr % 4
    half = (rr % 8) // 4
    q_g = [one_hot((cc == 64 + src_row) & (half == h)) for h in range(2)]
    q_t = one_hot(cc == src_row)
    rr2, cc2 = iota((64, 128), 0), iota((64, 128), 1)
    pick_tok = one_hot(cc2 == rr2)
    z2 = rr2 // 4
    for h in range(2):
        heads_in[h] = one_hot(cc2 == 8 * z2 + 4 * h + rr2 % 4)
        hid_in[h] = one_hot(cc2 == 64 * (z2 % 2) + 8 * (z2 // 2) + 4 * h + rr2 % 4)

    wire = Wire(send_sem, recv_sem, kv, tp)
    with jax.named_scope("barrier"):
        pl.semaphore_wait(barrier, (NZ - 1) + (NY - 1) + NY * (NT - 1))

    def y_send(group, buf, d, src=None):
        group.send(buf.at[y] if src is None else src, buf.at[y], kv_of(z, yp(d)), tp)

    g_tg, g_sm, g_mg = wire.group("g_tg"), wire.group("g_sm"), wire.group("g_mg")
    for d in (1, 3, 2):
        y_send(g_tg, tg, d, tg_s.at[yp(d)])
        y_send(g_sm, sm, d)
    for i in range(4):
        loads[7 + i].wait()
    full = (wqf, wkf, wvf, wgf)
    right = [wire.group("right") for _ in range(4)]
    left = [wire.group("left") for _ in range(4)]
    relay = [wire.group("relay") for _ in range(4)]
    for i in range(4):
        y_send(right[i], full[i], 1)
        y_send(left[i], full[i], 3)

    def pass_on(a, b):
        right[a].take(full[a].at[yp(-1)])
        relay[a].send(full[a].at[yp(-1)], full[a].at[yp(-1)], kv_of(z, yp(1)), tp)
        left[b].take(full[b].at[yp(1)])
        relay[b].send(full[b].at[yp(1)], full[b].at[yp(1)], kv_of(z, yp(-1)), tp)

    g_tg.take(tg.at[pl.ds(0, 3)])
    g_sm.take(sm.at[pl.ds(0, 3)])
    pass_on(0, 1)
    tgv = tg[...].reshape(256, 128)
    lq = [mm(q_g[h], tgv, NT_DIMS).astype(BF16) for h in range(2)]
    tok_rows = mm(pick_tok, tgv, NT_DIMS)

    t32 = tgv.astype(F32)
    energy = jnp.sum(t32 * t32, axis=0, keepdims=True)
    e_hi = energy.astype(BF16)
    e_lo = (energy - e_hi.astype(F32)).astype(BF16)
    e_rows = jnp.where(rr == 2, jnp.broadcast_to(e_hi.astype(F32), (128, 128)),
                       jnp.where(rr == 3, jnp.broadcast_to(e_lo.astype(F32), (128, 128)), 0.0)).astype(BF16)
    small_out = mm(q_t, e_rows, NT_DIMS)
    for h in range(2):
        sel = one_hot(((iota((128, 8), 0) == 0) & (iota((128, 8), 1) == h))
                      | ((iota((128, 8), 0) == 1) & (iota((128, 8), 1) == 2 + h)))
        parts = [mm(eye64, mm(sel, sm[yy]).astype(BF16), NT_DIMS) for yy in range(NY)]
        w_small = jnp.concatenate(parts, axis=0).astype(BF16)
        small_out += mm(lq[h], w_small)
    pass_on(2, 3)
    for i in range(11, 14):
        loads[i].wait()
    g_wo, g_wu, g_wu2 = wire.group("g_wo"), wire.group("g_wu"), wire.group("g_wu2")
    g_wd, g_wd2 = wire.group("g_wd"), wire.group("g_wd2")
    for d in (1, 3, 2):
        y_send(g_wo, wof, d)
    for d in (1, 3, 2):
        y_send(g_mg, mg, d)
    for d in (1, 3):
        y_send(g_wu, wuf, d)

    def project(buf):
        w = buf[...].reshape(256, 256)
        return mm(lq[0], w[:, :128]) + mm(lq[1], w[:, 128:])

    def stage(blocks):
        return jnp.concatenate([b.reshape(NZ, 8, 128) for b in blocks], axis=1).astype(BF16)

    def z_scatter(group, src, dst):
        for d in FAR_FIRST:
            group.send(src.at[zp(d)], dst.at[z], kv_of(zp(d), y), tp)

    def z_gather(group, buf):
        for d in FAR_FIRST:
            group.send(buf.at[z], buf.at[z], kv_of(zp(d), y), tp)

    def z_take(group, buf):
        group.take(buf.at[pl.ds(0, NZ - 1)])

    g_a, g_b, g_m = wire.group("g_a"), wire.group("g_b"), wire.group("g_m")
    left[0].take(wqf.at[yp(1)])
    relay[0].take(wqf.at[yp(2)])
    right[1].take(wkf.at[yp(-1)])
    relay[1].take(wkf.at[yp(2)])
    sa[...] = stage([project(wqf), project(wkf), small_out])
    z_scatter(g_a, sa, ra)
    left[2].take(wvf.at[yp(1)])
    relay[2].take(wvf.at[yp(2)])
    right[3].take(wgf.at[yp(-1)])
    relay[3].take(wgf.at[yp(2)])
    sb[...] = stage([project(wvf), project(wgf)])
    z_scatter(g_b, sb, rb)
    ra[pl.ds(z, 1)] = sa[pl.ds(z, 1)]
    rb[pl.ds(z, 1)] = sb[pl.ds(z, 1)]
    loads[14].wait()
    z_take(g_a, ra)
    sum_a = jnp.sum(ra[...].astype(F32), axis=0)
    extra = sum_a[16:24]
    scale = lax.rsqrt((extra[:, 2:3] + extra[:, 3:4]) * (1.0 / D) + EPS)
    query = jax.nn.silu(sum_a[0:8] * scale)
    query = query * lax.rsqrt(jnp.sum(query * query, axis=1, keepdims=True) + EPS) * (128 ** -0.5)
    keyed = jax.nn.silu(sum_a[8:16] * scale)
    keyed = keyed * lax.rsqrt(jnp.sum(keyed * keyed, axis=1, keepdims=True) + EPS)
    beta = jax.nn.sigmoid(extra[:, 0:1] * scale)
    rate = jnp.where(iota((8, 1), 0) < 4, ratev[0:1, 0:1], ratev[0:1, 1:2])
    decay = jnp.exp(-rate * jax.nn.softplus(extra[:, 1:2] * scale))
    key_t = jnp.transpose(keyed)
    query_t = jnp.transpose(query)
    recs = []
    for b in range(8):
        h, i = b // 4, b % 4
        recs.append(jnp.sum(st[i, h] * key_t[:, b:b + 1], axis=0, keepdims=True))
    recalled = jnp.concatenate(recs, axis=0)
    z_take(g_b, rb)
    sum_b = jnp.sum(rb[...].astype(F32), axis=0)
    valued = jax.nn.silu(sum_b[0:8] * scale)
    gate = jax.nn.silu(sum_b[8:16] * scale)
    write = beta * (valued - decay * recalled)
    reads = []
    for b in range(8):
        h, i = b // 4, b % 4
        fresh = decay[b:b + 1, :] * st[i, h] + key_t[:, b:b + 1] * write[b:b + 1, :]
        new_ref[i, h] = fresh
        reads.append(jnp.sum(fresh * query_t[:, b:b + 1], axis=0, keepdims=True))
    read = jnp.concatenate(reads, axis=0)
    mixed = read * lax.rsqrt(jnp.mean(read * read, axis=1, keepdims=True) + EPS) * hgainv[...] * gate
    mx[pl.ds(z, 1)] = mixed.astype(BF16)[None]
    z_gather(g_m, mx)

    def far_halves(group, buf):
        for from_y, at_row, to in ((yp(-1), 0, yp(1)), (yp(1), 32, yp(-1))):
            piece = buf.at[from_y, pl.ds(at_row, 32)]
            group.send(piece, piece, kv_of(z, to), tp)

    g_wu.take(wuf.at[pl.ds(0, 2)])
    far_halves(g_wu2, wuf)
    for d in (1, 3):
        y_send(g_wd, wdf, d)
    g_wo.take(wof.at[pl.ds(0, 3)])
    g_mg.take(mg.at[pl.ds(0, 3)])
    wov = wof[...].reshape(256, 256)
    z_take(g_m, mx)
    m = mx[...].astype(F32).reshape(128, 128).astype(BF16)
    mixed2 = jnp.concatenate([mm(heads_in[h], m) for h in range(2)], axis=1).astype(BF16)
    at[pl.ds(tp, 1)] = mm(mixed2, wov, NT_DIMS).astype(BF16)[None]
    g_t = wire.group("g_t")
    for d in (4, 5, 2, 3, 6, 7, 1):
        g_t.send(at.at[tp], at.at[tp], kv, tq(d))
    gain_mid = jnp.concatenate([mg[yy][0:1] for yy in range(NY)], axis=1)
    rr3, cc3 = iota((128, 64), 0), iota((128, 64), 1)
    row3 = 4 * (2 * ((rr3 % 64) // 8) + rr3 // 64) + rr3 % 4
    spread = [one_hot((cc3 == row3) & ((rr3 % 8) // 4 == c)) for c in range(2)]
    g_wu2.take(wuf.at[0])
    g_t.take(at.at[pl.ds(0, NT - 1)])
    attended = jnp.sum(at[...].astype(F32), axis=0)
    residual = (tok_rows + attended).astype(BF16)
    r32 = residual.astype(F32)
    gained_mid = (r32 * gain_mid).astype(BF16)
    lg = [mm(spread[c], gained_mid).astype(BF16) for c in range(2)]
    wu = wuf[...].reshape(256, 2048)
    g_u1, g_u2 = wire.group("g_u1"), wire.group("g_u2")
    par, m_here = z % 2, z // 2
    partner = (kv_of((z + 1 - 2 * par + NZ) % NZ, y), kv_of((z - 1 + 2 * par + NZ) % NZ, y))
    for f in range(2):
        lo, hi = 512 * f, 512 * (f + 1)
        up = mm(lg[0], wu[:, lo:hi]) + mm(lg[1], wu[:, 1024 + lo:1024 + hi])
        us[f] = up.reshape(2, 8, 8, 512).astype(BF16)
        g_u1.send(us.at[f, 1 - par], near.at[f], partner[f], tp)

    sq = r32 * r32
    sq_hi = sq.astype(BF16)
    sq_lo = (sq - sq_hi.astype(F32)).astype(BF16)
    ones = jnp.ones((8, 256), BF16)
    em[pl.ds(z, 1)] = (mm(ones, sq_hi, NT_DIMS) + mm(ones, sq_lo, NT_DIMS))[0:1][None]
    eye256 = one_hot(iota((256, 256), 0) == iota((256, 256), 1))

    def by_y(x):
        x = x.reshape(NY, 2, 32, 64)
        return jnp.concatenate([x[:, 0], x[:, 1]], axis=-1).astype(BF16)

    res_s[...] = by_y(mm(eye256, residual, NT_DIMS))
    res[pl.ds(y, 1)] = res_s[pl.ds(y, 1)]
    g_u1.take(near)
    def same_parity(e):
        return (m_here + e) % 8

    for f in range(2):
        pair = us[f, pl.ds(par, 1)][0].astype(F32) + near[f].astype(F32)
        fs[:, f] = pair.astype(BF16)
    for e in (4, 3, 5, 2, 6, 1, 7):
        g_u2.send(fs.at[same_parity(e)], ru.at[m_here], kv_of(2 * same_parity(e) + par, y), tp)
    ru[pl.ds(m_here, 1)] = fs[pl.ds(m_here, 1)]
    g_em, g_res = wire.group("g_em"), wire.group("g_res")
    z_gather(g_em, em)
    for d in (1, 3, 2):
        g_res.send(res_s.at[yp(d)], res.at[y], kv_of(z, yp(d)), tp)
    g_wd.take(wdf.at[pl.ds(0, 2)])
    far_halves(g_wd2, wdf)
    rr4, cc4 = iota((512, 256), 0), iota((512, 256), 1)
    row4 = 16 * ((rr4 % 64) // 4) + 4 * (rr4 // 128) + rr4 % 4
    for e in range(2):
        place[e] = one_hot((cc4 == row4) & ((rr4 % 128) // 64 == e))
    g_u2.take(ru.at[pl.ds(0, 7)])
    total = jnp.sum(ru[...].astype(F32), axis=0)
    hidden = jnp.square(jnp.maximum(total, 0.0)).astype(BF16)
    for f in range(2):
        hid[f, pl.ds(par, 1), pl.ds(m_here, 1)] = hidden[f][None, None]
    g_h1 = [wire.group("g_h1") for _ in range(7)]
    g_h2 = [wire.group("g_h2") for _ in range(2)]
    order = (4, 3, 5, 2, 6, 1, 7)
    for g, e in zip(g_h1, order):
        mine = hid.at[:, par, m_here]
        g.send(mine, mine, kv_of(2 * same_parity(e) + par, y), tp)

    def to_partners(slot):
        for f in range(2):
            piece = hid.at[f, par, slot]
            g_h2[f].send(piece, piece, partner[f], tp)

    to_partners(m_here)
    for g, e in zip(g_h1, order):
        g.take(hid.at[:, par, same_parity(8 - e)])
        to_partners(same_parity(8 - e))
    g_wd2.take(wdf.at[0])
    g_res.take(res.at[pl.ds(0, 3)])
    z_take(g_em, em)
    energy_mid = jnp.sum(em[...], axis=0)
    scale_mid = lax.rsqrt(energy_mid * (1.0 / D) + EPS)
    wd = wdf[...].reshape(256, 2048)
    for f in range(2):
        g_h2[f].take(hid.at[f, 1 - par])
    down = None
    for f in range(2):
        hv = hid[f].astype(F32).reshape(128, 512).astype(BF16)
        for c in range(2):
            rows = mm(hid_in[c], hv).astype(BF16)
            at_col = 1024 * c + 512 * f
            term = mm(wd[:, at_col:at_col + 512], rows, NT_DIMS)
            down = term if down is None else down + term
    fin_s[...] = by_y(down * (scale_mid * scale_mid))
    g_f = wire.group("g_f")
    for e in (2, 1, 3, 0):
        for d in (4, 5, 2, 3, 6, 7, 1, 0):
            if e == 0 and d == 0:
                continue
            g_f.send(fin_s.at[yp(e)], fin.at[tp * NY + y], kv_of(z, yp(e)), tq(d))
    fin[pl.ds(tp * NY + y, 1)] = fin_s[pl.ds(y, 1)]
    g_f.take(fin.at[pl.ds(0, 31)])
    mixer = jnp.sum(fin[...].astype(F32).reshape(NT, NY, 32, 128), axis=0)
    last = (res[...].astype(F32) + mixer).astype(BF16)
    flat = jnp.concatenate([last[yy] for yy in range(NY)], axis=1)
    for e in range(2):
        out_ref[pl.ds(32 * e, 32), :] = mm(flat, place[e]).astype(BF16)
    with jax.named_scope("finish"):
        wire.finish()


def body(
    tokens, mix_gain, w_query, w_key, w_value, w_gate, w_beta, w_decay, decay_rate, head_gain,
    state, w_out, mlp_gain, w_up, w_down,
):
    vmem = pl.BlockSpec(memory_space=pltpu.VMEM)
    hbm = pl.BlockSpec(memory_space=pltpu.HBM)
    v = pltpu.VMEM
    n_sem = 38
    out, new = pl.pallas_call(
        kernel,
        name="layer",
        out_shape=(
            pltpu.VMEM((64, 256), BF16),
            pltpu.VMEM((4, 2, 128, 128), F32),
        ),
        in_specs=[hbm] * 15,
        out_specs=(vmem, vmem),
        scratch_shapes=[
            v((64, 256), BF16), v((1, 64), F32), v((2, 64), BF16), v((2, 64), BF16),
            v((1, 2), F32), v((1, 128), F32), v((1, 64), F32),
            v((4, 64, 256), BF16), v((4, 64, 256), BF16), v((4, 64, 256), BF16), v((4, 64, 256), BF16),
            v((4, 64, 256), BF16), v((4, 64, 2048), BF16), v((4, 64, 2048), BF16),
            v((4, 2, 128, 128), F32),
            v((4, 64, 128), BF16), v((4, 64, 128), BF16), v((4, 8, 64), BF16), v((4, 8, 64), F32),
            v((16, 24, 128), BF16), v((16, 16, 128), BF16), v((16, 24, 128), BF16), v((16, 16, 128), BF16),
            v((16, 8, 128), BF16), v((8, 64, 256), BF16),
            v((2, 2, 8, 8, 512), BF16), v((2, 8, 8, 512), BF16), v((8, 2, 8, 512), BF16), v((8, 2, 8, 512), BF16),
            v((2, 2, 8, 8, 512), BF16), v((16, 1, 64), F32),
            v((4, 32, 128), BF16), v((4, 32, 128), BF16),
            v((4, 32, 128), BF16), v((32, 32, 128), BF16),
            v((2, 64, 128), BF16), v((2, 64, 128), BF16), v((2, 512, 256), BF16),
            pltpu.SemaphoreType.DMA((n_sem,)), pltpu.SemaphoreType.DMA((n_sem,)),
            pltpu.SemaphoreType.DMA((15,)),
        ],
        compiler_params=pltpu.CompilerParams(
            collective_id=0, has_side_effects=True, vmem_limit_bytes=66000000,
        ),
    )(
        tokens.T, mix_gain.reshape(1, 64), w_query, w_key, w_value, w_gate,
        w_beta.T, w_decay.T, decay_rate.reshape(1, 2), head_gain.reshape(1, 128), state, w_out.T,
        mlp_gain.reshape(1, 64), w_up, w_down.T,
    )
    return out.T, new


def solution(mesh):
    return jax.shard_map(
        body,
        mesh=mesh,
        in_specs=(
            P(None, "kv"), P("kv"), P("kv", "tp"), P("kv", "tp"), P("kv", "tp"), P("kv", "tp"),
            P("kv", "tp"), P("kv", "tp"), P("tp"), P(), P("kv", "tp", None, None),
            P("tp", "kv"), P("kv"), P("kv", "tp"), P("tp", "kv"),
        ),
        out_specs=(P(None, "kv"), P("kv", "tp", None, None)),
        check_vma=False,
    )
```

time: 101 us -> 81.9 us (0.81)
  Pallas kernels: 88.4 us -> 79.7 us
  local copies, waits for them, and re-layouts: 9.69 us -> 1.41 us
  other arithmetic: 1.62 us -> 0 us
    pallas_call x1, Pallas kernels: 88.4 us -> 79.7 us  [body(): pl.pallas_call(kernel, name='layer', out_shape=(pltpu.VMEM((64, 256), BF1...]
    unnamed x24 -> x2, local copies, waits for them, and re-layouts: 8.73 us -> 1.41 us
    concatenate x2 -> x0, other arithmetic: 1.62 us -> none  [the longest x1 0.88 us: body(): gain4 = jnp.concatenate([mlp_gain] * 4).reshape(1, 256)]
where the time goes in v2:
time: 81.9 us; the launch traced here: 81.8 us
  Pallas kernels  79.7 us (97%)
  local copies, waits for them, and re-layouts  1.41 us (2%)
    pallas_call x1, Pallas kernels, body(): pl.pallas_call(kernel, name='layer', out_shape=(pltpu.VMEM((64, 256), BF1...  79.7 us

profile of v2, /device:TPU:1, one launch (start us, length us, event | category | flops | bytes accessed | tf_op | source)
XLA Modules:
  0.0 81.8 jit_solution(1096498930148878792)
XLA Ops:
  0.6 79.7 %layer.1 = (bf16[64,256]{1,0:T(8,128)(2,1)S(1)}, f32[4,2,128,128]{3,2,1,0:T(8,128)S(1)}) custom-call(bf16[64,256]{1,0:T(8,128)(2,1)} %bitcast.12, f32[1,64]{1,0:T(1,128)} %bitcast.14, bf16[64,256]{1,0:T(8,128)(2,1)} %wq_ref.1, bf16[64,256]{1,0:T(8,128)(2,1)} %wk_ref.1, bf16[64,256]{1,0:T(8,128)(2,1)} %wv_ref.1, bf16[64,256]{1,0:T(8,128)(2,1)} %wg_ref.1, ...), custom_call_target="tpu_custom_call" | custom-call | tf_op jit(solution)/shard_map/layer/pallas_call | solution.py:415
  80.4 0.6 copy.19
  81.0 0.8 copy.20

commit v3 on v2

--- a/solution.py
+++ b/solution.py
@@ -74,7 +74,7 @@
     tokv, mixv, wbv, wdecv, ratev, hgainv, mlpv,
     wqf, wkf, wvf, wgf, wof, wuf, wdf, st,
     tg_s, tg, sm, mg, sa, sb, ra, rb, mx, at, us, near, fs, ru, hid, em, res_s, res, fin_s, fin,
-    heads_in, hid_in, place, send_sem, recv_sem, local_sem,
+    heads_in, hid_in, place, send_sem, recv_sem, local_sem, known,
 ):
     kv, tp = lax.axis_index("kv"), lax.axis_index("tp")
     z, y = kv // NY, kv % NY
@@ -91,14 +91,20 @@
     def tq(d):
         return (tp + d) % NT
 
+    def notify(sem, kv_t, tp_t):
+        pl.semaphore_signal(sem, 1, device_id={"kv": kv_t, "tp": tp_t}, device_id_type=MESH)
+
+    def partner_core():
+        return tp + 1 - 2 * (tp % 2)
+
     barrier = pltpu.get_barrier_semaphore()
-    for d in range(1, NZ):
-        pl.semaphore_signal(barrier, 1, device_id={"kv": kv_of(zp(d), y), "tp": tp}, device_id_type=MESH)
-    for d in range(1, NY):
-        pl.semaphore_signal(barrier, 1, device_id={"kv": kv_of(z, yp(d)), "tp": tp}, device_id_type=MESH)
-    for e in range(NY):
-        for d in range(1, NT):
-            pl.semaphore_signal(barrier, 1, device_id={"kv": kv_of(z, yp(e)), "tp": tq(d)}, device_id_type=MESH)
+    for d in (1, NZ - 1):
+        notify(barrier, kv_of(zp(d), y), tp)
+    for d in (2, 1, 3):
+        notify(barrier, kv_of(z, yp(d)), tp)
+    for d in (4, 2, 6):
+        notify(barrier, kv, tq(d))
+    notify(barrier, kv, partner_core())
 
     loads = []
     for i, (src, dst) in enumerate((
@@ -151,7 +157,11 @@
 
     wire = Wire(send_sem, recv_sem, kv, tp)
     with jax.named_scope("barrier"):
-        pl.semaphore_wait(barrier, (NZ - 1) + (NY - 1) + NY * (NT - 1))
+        pl.semaphore_wait(barrier, 9)
+    for d in (1, NZ - 1):
+        notify(known.at[0], kv_of(zp(d), y), tp)
+    for d in range(1, NY):
+        notify(known.at[1], kv_of(z, yp(d)), tp)
 
     def y_send(group, buf, d, src=None):
         group.send(buf.at[y] if src is None else src, buf.at[y], kv_of(z, yp(d)), tp)
@@ -169,6 +179,13 @@
     for i in range(4):
         y_send(right[i], full[i], 1)
         y_send(left[i], full[i], 3)
+    with jax.named_scope("known0"):
+        pl.semaphore_wait(known.at[0], 2)
+    for d in (2, NZ - 2):
+        notify(known.at[2], kv_of(zp(d), y), tp)
+    with jax.named_scope("known1"):
+        pl.semaphore_wait(known.at[1], NY - 1)
+    notify(known.at[3], kv, partner_core())
 
     def pass_on(a, b):
         right[a].take(full[a].at[yp(-1)])
@@ -178,6 +195,10 @@
 
     g_tg.take(tg.at[pl.ds(0, 3)])
     g_sm.take(sm.at[pl.ds(0, 3)])
+    with jax.named_scope("known2"):
+        pl.semaphore_wait(known.at[2], 2)
+    for d in (4, NZ - 4):
+        notify(known.at[4], kv_of(zp(d), y), tp)
     pass_on(0, 1)
     tgv = tg[...].reshape(256, 128)
     lq = [mm(q_g[h], tgv, NT_DIMS).astype(BF16) for h in range(2)]
@@ -197,6 +218,9 @@
         w_small = jnp.concatenate(parts, axis=0).astype(BF16)
         small_out += mm(lq[h], w_small)
     pass_on(2, 3)
+    with jax.named_scope("known3"):
+        pl.semaphore_wait(known.at[3], 1)
+        pl.semaphore_wait(known.at[4], 2)
     for i in range(11, 14):
         loads[i].wait()
     g_wo, g_wu, g_wu2 = wire.group("g_wo"), wire.group("g_wu"), wire.group("g_wu2")
@@ -436,7 +460,7 @@
             v((4, 32, 128), BF16), v((32, 32, 128), BF16),
             v((2, 64, 128), BF16), v((2, 64, 128), BF16), v((2, 512, 256), BF16),
             pltpu.SemaphoreType.DMA((n_sem,)), pltpu.SemaphoreType.DMA((n_sem,)),
-            pltpu.SemaphoreType.DMA((15,)),
+            pltpu.SemaphoreType.DMA((15,)), pltpu.SemaphoreType.REGULAR((5,)),
         ],
         compiler_params=pltpu.CompilerParams(
             collective_id=0, has_side_effects=True, vmem_limit_bytes=66000000,

time: 81.9 us -> 77.7 us (0.949)
  Pallas kernels: 79.7 us -> 75.5 us
    pallas_call x1, Pallas kernels: 79.7 us -> 75.5 us  [body(): pl.pallas_call(kernel, name='layer', out_shape=(pltpu.VMEM((64, 256), BF1...]
where the time goes in v3:
time: 77.7 us; the launch traced here: 77.5 us
  Pallas kernels  75.5 us (97%)
  local copies, waits for them, and re-layouts  1.41 us (2%)
    pallas_call x1, Pallas kernels, body(): pl.pallas_call(kernel, name='layer', out_shape=(pltpu.VMEM((64, 256), BF1...  75.5 us

profile of v3, /device:TPU:1, one launch (start us, length us, event | category | flops | bytes accessed | tf_op | source)
XLA Modules:
  0.0 77.5 jit_solution(4844942132905107430)
XLA Ops:
  0.6 75.5 %layer.1 = (bf16[64,256]{1,0:T(8,128)(2,1)S(1)}, f32[4,2,128,128]{3,2,1,0:T(8,128)S(1)}) custom-call(bf16[64,256]{1,0:T(8,128)(2,1)} %bitcast.12, f32[1,64]{1,0:T(1,128)} %bitcast.14, bf16[64,256]{1,0:T(8,128)(2,1)} %wq_ref.1, bf16[64,256]{1,0:T(8,128)(2,1)} %wk_ref.1, bf16[64,256]{1,0:T(8,128)(2,1)} %wv_ref.1, bf16[64,256]{1,0:T(8,128)(2,1)} %wg_ref.1, ...), custom_call_target="tpu_custom_call" | custom-call | tf_op jit(solution)/shard_map/layer/pallas_call | solution.py:439
  76.1 0.6 copy.19
  76.8 0.8 %copy.20 = f32[4,2,128,128]{3,2,1,0:T(8,128)} copy(f32[4,2,128,128]{3,2,1,0:T(8,128)S(1)} %get-tuple-element.7) | data formatting | bytes 1048576
